TPU v7x, 32 devices: a whole 2x2x4 slice. The times are simulated.
32 devices in a mesh: ep: 8 (over z, core), tp: 4 (over y, x).
Axes of the slice: x: 2, y: 2, z: 4, core: 2. Of those that a mesh axis runs over, the one named last changes fastest.
Arguments:
- gate_out: bfloat16 [2048, 1024], P('ep', 'tp'), may hold values from -6 to 6
- gate_in: bfloat16 [2048, 1024], P('ep', 'tp'), may hold values from -6 to 6
- conv_values: bfloat16 [2048, 1024], P('ep', 'tp'), may hold values from -6 to 6
- conv_taps: float32 [3, 1024], P(None, 'tp'), may hold values from -3 to 3
- mixer_proj: bfloat16 [1024, 2048], P('tp'), may hold values from -0.25 to 0.25
- expert_in: bfloat16 [2048, 2048], P('ep'), may hold values from -6 to 6
- norm_gain: float32 [2048], replicated, may hold values from 0.1 to 1.9
- route_ids: int32 [2048, 2], P('ep'), may hold values from 0 to 7, all different within a row; in each aligned block of 256 rows (0 to 255, 256 to 511, ...) at most 86 rows name the same one
- route_scores: float32 [2048, 2], P('ep'), may hold values from 0.1 to 1
- gate_proj: bfloat16 [8, 2048, 4096], P('ep', None, 'tp'), may hold values from -0.125 to 0.125
- up_proj: bfloat16 [8, 2048, 4096], P('ep', None, 'tp'), may hold values from -0.125 to 0.125
- down_proj: bfloat16 [8, 4096, 2048], P('ep', 'tp'), may hold values from -0.125 to 0.125
Outputs:
- mixed: bfloat16 [2048, 2048], P('ep', 'tp')
- expert_mix: bfloat16 [2048, 2048], P('ep', 'tp')
Inputs may be any that keep to these rules, and one draw needn't show every extreme that they name: `route_ids`: each row names 2 different experts. Within each aligned block of 256 rows (the rows of one device of ep) no expert is named by more than 86 rows, and in some block an expert is named by exactly 86 rows.
All inputs are finite; a program needn't handle non-finite values.
Results may differ from a plain program's by a relative error of at most 0.015.
Values may be sent and summed in bfloat16 or wider, within the bound.
A program may use at most 64 MiB of HBM per device.

v0:
```python
import jax
import jax.numpy as jnp
from jax import lax
from jax.sharding import PartitionSpec as P


def shifted(block, axis, distance):
    devices = range(lax.axis_size(axis))
    route = [(i - distance, i) for i in devices if i - distance in devices]
    return lax.ppermute(block, axis, route)


def slot_table(route_ids, experts_total, capacity):
    pairs = route_ids.reshape(-1)
    onehot = (pairs[:, None] == jnp.arange(experts_total, dtype=jnp.int32)[None, :]).astype(
        jnp.int32
    )
    before = jnp.cumsum(onehot, axis=0) - onehot
    ranking = jnp.sum(before * onehot, axis=1)
    return (pairs * capacity + ranking).reshape(route_ids.shape)


def shards(
    gate_out,
    gate_in,
    conv_values,
    conv_taps,
    mixer_proj,
    expert_in,
    norm_gain,
    route_ids,
    route_scores,
    gate_proj,
    up_proj,
    down_proj,
):
    product = gate_in.astype(jnp.float32) * conv_values.astype(jnp.float32)
    seq_len = product.shape[0]
    tap_count = conv_taps.shape[0]
    earlier = shifted(product[seq_len - (tap_count - 1) :], "ep", 1)
    padded = jnp.concatenate([earlier, product], axis=0)
    convolved = conv_taps[0] * padded[0:seq_len]
    for offset in range(1, tap_count):
        convolved = convolved + conv_taps[offset] * padded[offset : offset + seq_len]
    branch = (gate_out.astype(jnp.float32) * convolved).astype(jnp.bfloat16)
    partial_mix = jnp.dot(branch, mixer_proj, preferred_element_type=jnp.float32)
    mixed = lax.psum_scatter(
        partial_mix.astype(jnp.bfloat16), "tp", scatter_dimension=1, tiled=True
    )
    rows_wide = expert_in.astype(jnp.float32)
    scaling = lax.rsqrt(jnp.mean(rows_wide * rows_wide, axis=1, keepdims=True) + 1e-06)
    normed = (rows_wide * scaling * norm_gain).astype(jnp.bfloat16)
    token_count = expert_in.shape[0]
    choose_count = route_ids.shape[1]
    model_width = expert_in.shape[1]
    ep_count = lax.axis_size("ep")
    local_experts = gate_proj.shape[0]
    experts_total = ep_count * local_experts
    capacity = max(
        2, (4 * token_count * choose_count + 3 * experts_total - 1) // (3 * experts_total)
    )
    slot_count = experts_total * capacity
    slots = slot_table(route_ids, experts_total, capacity)
    hits = slots[None, :, :] == jnp.arange(slot_count, dtype=jnp.int32)[:, None, None]
    dispatch = jnp.sum(hits.astype(jnp.int32), axis=2).astype(jnp.bfloat16)
    column_count = model_width // lax.axis_size("tp")
    own_columns = lax.dynamic_slice_in_dim(
        normed, lax.axis_index("tp") * column_count, column_count, 1
    )
    sent = jnp.dot(dispatch, own_columns, preferred_element_type=jnp.float32).astype(jnp.bfloat16)
    arrived = lax.all_to_all(sent, "ep", split_axis=0, concat_axis=0, tiled=True)
    piece = lax.all_gather(arrived, "tp", axis=1, tiled=True)
    grouped_piece = piece.reshape(ep_count, local_experts, capacity, piece.shape[1])
    gate_part = jnp.einsum(
        "secd,edf->secf", grouped_piece, gate_proj, preferred_element_type=jnp.float32
    )
    up_part = jnp.einsum(
        "secd,edf->secf", grouped_piece, up_proj, preferred_element_type=jnp.float32
    )
    hidden = (jax.nn.silu(gate_part) * up_part).astype(jnp.bfloat16)
    partial_out = jnp.einsum(
        "secf,efd->secd", hidden, down_proj, preferred_element_type=jnp.float32
    )
    summed = lax.psum_scatter(
        partial_out.astype(jnp.bfloat16), "tp", scatter_dimension=3, tiled=True
    )
    returned = lax.all_to_all(summed, "ep", split_axis=0, concat_axis=0, tiled=True)
    slot_rows = returned.reshape(slot_count, returned.shape[3])
    picked = jnp.take(slot_rows, slots.reshape(-1), axis=0).reshape(
        token_count, choose_count, slot_rows.shape[1]
    )
    weights = route_scores / jnp.sum(route_scores, axis=1, keepdims=True)
    expert_mix = jnp.sum(weights[:, :, None] * picked.astype(jnp.float32), axis=1).astype(
        jnp.bfloat16
    )
    return (mixed, expert_mix)


def solution(mesh):
    placed = (
        P("ep", "tp"),
        P("ep", "tp"),
        P("ep", "tp"),
        P(None, "tp"),
        P("tp", None),
        P("ep", None),
        P(),
        P("ep", None),
        P("ep", None),
        P("ep", None, "tp"),
        P("ep", None, "tp"),
        P("ep", "tp", None),
    )
    return jax.shard_map(
        shards,
        mesh=mesh,
        in_specs=placed,
        out_specs=(P("ep", "tp"), P("ep", "tp")),
        check_vma=False,
    )
```

profile of v0, /device:TPU:16, one launch (start us, length us, event | category | flops | bytes accessed | tf_op | source)
XLA Modules:
  0.0 185.4 jit_solution(16390596745611525684)
XLA Ops:
  7.2 0.0 copy-start
  7.2 0.0 copy-start.5
  7.2 0.0 copy-start.1
  7.2 0.0 all-gather.2.cloned.1.call-start
  7.2 0.9 copy.33
  8.2 0.1 eq.39
  8.3 0.1 reshape.111
  8.5 2.8 %convert_element_type.67 = f32[256,2048]{1,0:T(8,128)} convert(bf16[256,2048]{1,0:T(8,128)(2,1)} %param.17) | non-fusion elementwise | flops 524288 | bytes 3145728 | tf_op jit(solution)/shard_map/convert_element_type | solution.py:50
  11.3 0.0 copy-done.1
  11.3 0.3 multiply_reduce_fusion
  11.6 1.1 reduce-window.6
  12.8 0.2 slice_reduce_fusion
  13.0 0.1 fusion.41
  13.1 0.1 reduce_sum.51
  13.3 0.1 copy.35
  13.4 0.3 convert_reduce_fusion
  13.7 0.8 dynamic-slice
  14.4 1.5 convolution_convert_fusion.1
  15.9 0.2 all_to_all.11
  16.1 21.4 %all_to_all.17 = bf16[8,86,512]{2,1,0:T(8,128)(2,1)S(1)} all-to-all(bf16[8,86,512]{2,1,0:T(8,128)(2,1)S(1)} %all_to_all.11), channel_id=1, replica_groups=mesh['ep'=8,'tp'=4] {'ep'}, dimensions={0} | all-to-all | bytes 1409024 | tf_op jit(solution)/shard_map/all_to_all | solution.py:71
  37.5 1.1 all_to_all.13
  38.6 0.0 all-gather.2.cloned.1.call-update
  38.6 0.0 reduce-scatter.5.cloned.1.call-start
  38.7 42.6 %all-gather.2.cloned.1.call-done = bf16[688,2048]{1,0:T(8,128)(2,1)} async-done(((bf16[688,512]{1,0:T(8,128)(2,1)}), bf16[688,2048]{1,0:T(8,128)(2,1)}) %all-gather.2.cloned.1.call-update) | async-done | bytes 2818064 | tf_op jit(solution)/shard_map/all_gather | solution.py:72
  81.3 3.3 %reshape.113 = bf16[8,86,2048]{2,1,0:T(8,128)(2,1)} reshape(bf16[688,2048]{1,0:T(8,128)(2,1)} %all-gather.2.cloned.1.call-done) | data formatting | bytes 5636096 | tf_op jit(solution)/shard_map/reshape.9
  84.7 7.8 %fusion.2 = f32[8,86,1024]{2,1,0:T(8,128)} fusion(bf16[8,86,2048]{2,1,0:T(8,128)(2,1)} %reshape.113, bf16[1,2048,1024]{2,1,0:T(8,128)(2,1)} %param.22), kind=kOutput, calls=%fused_computation.3 | convolution fusion | flops 2885681152 | bytes 9830400 | tf_op jit(solution)/shard_map/secd,edf->secf/dot_general | solution.py:77
  92.4 13.0 %fusion.9 = bf16[8,1,86,2048]{3,2,0,1:T(8,128)(2,1)} fusion(bf16[1,1024,2048]{2,1,0:T(8,128)(2,1)} %param.23, f32[8,86,1024]{2,1,0:T(8,128)} %fusion.2, bf16[8,86,2048]{2,1,0:T(8,128)(2,1)} %reshape.113, bf16[1,2048,1024]{2,1,0:T(8,128)(2,1)} %param.21), kind=kOutput, calls=%fused_computation.8 | convolution fusion | flops 5776998400 | bytes 16842752 | tf_op jit(solution)/shard_map/secf,efd->secd/dot_general | solution.py:81
  105.5 0.0 reduce-scatter.5.cloned.1.call-update
  105.5 0.0 copy-start.6
  105.5 0.0 reduce-scatter.3.cloned.1.call-start
  105.6 0.8 copy-done.3
  106.4 0.1 copy-done.4
  106.5 1.9 %collective-permute-start = (f32[2,256]{1,0:T(2,128)S(1)}, f32[2,256]{1,0:T(2,128)S(1)}, u32[]{:S(2)}, u32[]{:S(2)}) collective-permute-start(f32[2,256]{1,0:T(2,128)S(1)} %slice.34), channel_id=1, source_target_pairs={{0,4},{4,8},{8,12},{12,16},{16,20},{20,24},{24,28},{1,5},{5,9},{9,... | collective-permute-start | bytes 6152 | tf_op jit(solution)/shard_map/ppermute | solution.py:10
  108.4 3.0 %collective-permute-done = f32[2,256]{1,0:T(2,128)S(1)} collective-permute-done((f32[2,256]{1,0:T(2,128)S(1)}, f32[2,256]{1,0:T(2,128)S(1)}, u32[]{:S(2)}, u32[]{:S(2)}) %collective-permute-start) | collective-permute-done | bytes 2080 | tf_op jit(solution)/shard_map/ppermute | solution.py:10
  111.4 1.4 convolution_convert_fusion
  112.8 0.0 reduce-scatter.3.cloned.1.call-update
  112.9 34.5 %reduce-scatter.5.cloned.1.call-done = bf16[8,1,86,512]{3,2,0,1:T(8,128)(2,1)} async-done(((bf16[8,1,86,2048]{3,2,0,1:T(8,128)(2,1)}), bf16[8,1,86,512]{3,2,0,1:T(8,128)(2,1)}) %reduce-scatter.5.cloned.1.call-update) | async-done | bytes 704528 | tf_op jit(solution)/shard_map/reduce_scatter | solution.py:84
  147.4 5.1 %all-to-all-start.1 = ((bf16[8,1,86,512]{3,2,1,0:T(8,128)(2,1)}), bf16[8,1,86,512]{3,2,1,0:T(8,128)(2,1)S(1)}, u32[]{:S(2)}, u32[]{:S(2)}) async-start(bf16[8,1,86,512]{3,2,1,0:T(8,128)(2,1)} %bitcast.82), calls=%async_computation.3 | async-start | bytes 1441792 | tf_op jit(solution)/shard_map/all_to_all | solution.py:87
  152.5 0.1 copy.38
  152.7 0.1 mul.120
  152.8 0.2 copy.36
  153.0 0.1 copy.32
  153.2 15.6 %all-to-all-done.1 = bf16[8,1,86,512]{3,2,1,0:T(8,128)(2,1)S(1)} async-done(((bf16[8,1,86,512]{3,2,1,0:T(8,128)(2,1)}), bf16[8,1,86,512]{3,2,1,0:T(8,128)(2,1)S(1)}, u32[]{:S(2)}, u32[]{:S(2)}) %all-to-all-start.1) | async-done | bytes 704544 | tf_op jit(solution)/shard_map/all_to_all | solution.py:87
  168.8 0.2 reshape.118
  169.0 2.0 %gather_fusion = bf16[512,512]{1,0:T(8,128)(2,1)S(1)} fusion(bf16[688,512]{1,0:T(8,128)(2,1)S(1)} %reshape.118, s32[1024]{0:T(1024)S(1)} %pad_clamp_fusion), kind=kCustom, calls=%fused_computation | custom fusion | bytes 1050624 | tf_op jit(solution)/shard_map/jit(_take)/gather | solution.py:89
  170.9 0.2 gather.7
  171.2 2.9 %multiply_reduce_fusion.1 = bf16[256,512]{1,0:T(8,128)(2,1)} fusion(bf16[256,2,512]{2,1,0:T(2,128)(2,1)S(1)} %gather.7, pred[256,2]{1,0:T(8,128)(4,1)S(1)} %copy.36, f32[256,2]{1,0:T(8,128)S(1)} %copy.32), kind=kLoop, calls=%fused_computation.22 | loop fusion | flops 917504 | bytes 788992 | tf_op jit(solution)/shard_map/reduce_sum | solution.py:93
  174.1 4.8 %reduce-scatter.3.cloned.1.call-done = bf16[256,512]{1,0:T(8,128)(2,1)} async-done(((bf16[256,2048]{1,0:T(8,128)(2,1)}), bf16[256,512]{1,0:T(8,128)(2,1)}) %reduce-scatter.3.cloned.1.call-update) | async-done | bytes 262160 | tf_op jit(solution)/shard_map/reduce_scatter | solution.py:47
  (22 shorter events, 0.2 us)
Async XLA Ops:
  7.2 104.2 %copy-start = (bf16[256,2048]{1,0:T(8,128)(2,1)S(1)}, bf16[256,2048]{1,0:T(8,128)(2,1)}, u32[]{:S(2)}) copy-start(bf16[256,2048]{1,0:T(8,128)(2,1)} %param.16) | copy-start | bytes 3145732
  7.2 6.2 %copy-start.5 = (s32[256,2]{0,1:T(2,128)S(1)}, s32[256,2]{0,1:T(2,128)}, u32[]{:S(2)}) copy-start(s32[256,2]{0,1:T(2,128)} %param.19) | copy-start | bytes 6148
  7.2 4.1 %copy-start.1 = (bf16[256,2048]{1,0:T(8,128)(2,1)S(1)}, bf16[256,2048]{1,0:T(8,128)(2,1)}, u32[]{:S(2)}) copy-start(bf16[256,2048]{1,0:T(8,128)(2,1)} %param.17) | copy-start | bytes 3145732
  7.2 74.1 %all-gather.2.cloned.1.call-start = ((), (), s32[]{:S(2)}) async-start(), calls=%async_computation.5 | async-start | bytes 3522560 | tf_op jit(solution)/shard_map/all_gather | solution.py:72
  38.6 108.8 %reduce-scatter.5.cloned.1.call-start = ((), (), s32[]{:S(2)}) async-start(), calls=%async_computation.6 | async-start | bytes 3604480 | tf_op jit(solution)/shard_map/reduce_scatter | solution.py:84
  105.5 0.9 copy-start.3
  105.5 1.0 copy-start.4
  105.5 2.9 %copy-start.7 = (f32[3,256]{1,0:T(4,128)S(1)}, f32[3,256]{1,0:T(4,128)}, u32[]{:S(2)}) copy-start(f32[3,256]{1,0:T(4,128)} %param.15) | copy-start | bytes 9220
  105.5 5.9 %copy-start.2 = (bf16[256,256]{1,0:T(8,128)(2,1)S(1)}, bf16[256,256]{1,0:T(8,128)(2,1)}, u32[]{:S(2)}) copy-start(bf16[256,256]{1,0:T(8,128)(2,1)} %param.12) | copy-start | bytes 393220
  105.5 47.5 %copy-start.6 = (f32[256,2]{0,1:T(2,128)S(1)}, f32[256,2]{0,1:T(2,128)}, u32[]{:S(2)}) copy-start(f32[256,2]{0,1:T(2,128)} %param.20) | copy-start | bytes 6148
  105.5 73.3 %reduce-scatter.3.cloned.1.call-start = ((), (), s32[]{:S(2)}) async-start(), calls=%async_computation.4 | async-start | bytes 1310720 | tf_op jit(solution)/shard_map/reduce_scatter | solution.py:47
  106.5 4.9 %collective-permute-start = (f32[2,256]{1,0:T(2,128)S(1)}, f32[2,256]{1,0:T(2,128)S(1)}, u32[]{:S(2)}, u32[]{:S(2)}) collective-permute-start(f32[2,256]{1,0:T(2,128)S(1)} %slice.34), channel_id=1, source_target_pairs={{0,4},{4,8},{8,12},{12,16},{16,20},{20,24},{24,28},{1,5},{5,9},{9,... | collective-permute-start | bytes 6152 | tf_op jit(solution)/shard_map/ppermute | solution.py:10
  147.4 21.4 %all-to-all-start.1 = ((bf16[8,1,86,512]{3,2,1,0:T(8,128)(2,1)}), bf16[8,1,86,512]{3,2,1,0:T(8,128)(2,1)S(1)}, u32[]{:S(2)}, u32[]{:S(2)}) async-start(bf16[8,1,86,512]{3,2,1,0:T(8,128)(2,1)} %bitcast.82), calls=%async_computation.3 | async-start | bytes 1441792 | tf_op jit(solution)/shard_map/all_to_all | solution.py:87
Sparse Core Ops, SparseCore 0:
  38.7 42.5 all-gather.1
  105.6 41.7 reduce-scatter.4
  150.9 27.9 reduce-scatter.2
where the time goes:
time: 187 us; the launch traced here: 185 us
  waiting for transfers between devices  100 us (53%)
  matrix products  23.7 us (13%)
  blocking collectives  21.4 us (11%)
  between operations  14 us (7%)
  local copies, waits for them, and re-layouts  10.9 us (6%)
  other arithmetic  7.69 us (4%)
  starting transfers between devices  7.16 us (4%)
    all_gather x1, waiting for transfers between devices, shards(): piece = lax.all_gather(arrived, 'tp', axis=1, tiled=True)  42.6 us
    reduce_scatter x1, waiting for transfers between devices, shards(): lax.psum_scatter(partial_out.astype(jnp.bfloat16), 'tp', scatter_dimensio...  34.5 us
    all_to_all x1, blocking collectives, shards(): lax.all_to_all(sent, 'ep', split_axis=0, concat_axis=0, tiled=True)  21.4 us
    all_to_all x1, waiting for transfers between devices, shards(): lax.all_to_all(summed, 'ep', split_axis=0, concat_axis=0, tiled=True)  15.6 us
    dot_general x1, matrix products, shards(): jnp.einsum('secf,efd->secd', hidden, down_proj, preferred_element_type=jn...  13 us
    dot_general x1, matrix products, shards(): jnp.einsum('secd,edf->secf', grouped_piece, up_proj, preferred_element_ty...  7.78 us
    all_to_all x1, starting transfers between devices, shards(): lax.all_to_all(summed, 'ep', split_axis=0, concat_axis=0, tiled=True)  5.12 us
    reduce_scatter x1, waiting for transfers between devices, shards(): lax.psum_scatter(partial_mix.astype(jnp.bfloat16), 'tp', scatter_dimensio...  4.76 us
  transfers between devices with their start and end apart: 5, of which 5 were waited for; matrix products, arithmetic and copies ran while one was open for 4% of the time, Pallas kernels for 0%

commit v1 on v0

v1 whole, which is shorter than its diff:
```python
import functools

import jax
import jax.numpy as jnp
from jax import lax
from jax.experimental import pallas as pl
from jax.experimental.pallas import tpu as pltpu
from jax.sharding import PartitionSpec as P

BF16 = jnp.bfloat16
F32 = jnp.float32


def round_up(value, unit):
    return -(-value // unit) * unit


def partner(index, mask):
    bit = 1
    while bit <= mask:
        if mask & bit:
            index = index + bit - 2 * bit * ((index // bit) % 2)
        bit *= 2
    return index


def kernel(
    sizes,
    gate_out,
    gate_in,
    conv_values,
    taps,
    expert_in,
    gain,
    route_ids,
    scores,
    mixer_hbm,
    gate_hbm,
    up_hbm,
    down_hbm,
    mixed,
    expert_mix,
    mixer_w,
    gate_w,
    up_w,
    down_w,
    padded,
    halo,
    product_tail,
    mix_part,
    mix_recv,
    send_rows,
    rows,
    hidden,
    part,
    recv,
    summed,
    back,
    pick,
    weight_sem,
    halo_sem,
    mix_send_sem,
    mix_recv_sem,
    disp_send_sem,
    disp_recv_sem,
    gather_send_sem,
    gather_recv_sem,
    part_send_sem,
    part_recv_sem,
    back_send_sem,
    back_recv_sem,
):
    n_ep, n_tp, slots, width = sizes
    group = 2 if n_ep % 2 == 0 else 1
    while group * slots < 128 and group * 2 <= n_ep:
        group *= 2
    chunks = n_ep // group
    span = group * slots
    ep = lax.axis_index("ep")
    tp = lax.axis_index("tp")
    tokens = expert_in.shape[0]
    model = expert_in.shape[1]
    own = pl.ds(pl.multiple_of(tp * width, width), width)

    def ep_peer(p):
        return {"ep": partner(ep, p)}

    def tp_peer(q):
        return {"tp": partner(tp, q)}

    def remote(src, dst, send, recv, device):
        return pltpu.make_async_remote_copy(
            src_ref=src,
            dst_ref=dst,
            send_sem=send,
            recv_sem=recv,
            device_id=device,
            device_id_type=pl.DeviceIdType.MESH,
        )

    barrier = pltpu.get_barrier_semaphore()
    for p in range(1, n_ep):
        pl.semaphore_signal(barrier, inc=1, device_id=ep_peer(p), device_id_type=pl.DeviceIdType.MESH)
    for q in range(1, n_tp):
        pl.semaphore_signal(barrier, inc=1, device_id=tp_peer(q), device_id_type=pl.DeviceIdType.MESH)

    loads = [
        pltpu.make_async_copy(src, dst, weight_sem.at[i])
        for i, (src, dst) in enumerate(
            [(mixer_hbm, mixer_w), (gate_hbm, gate_w), (up_hbm, up_w), (down_hbm, down_w)]
        )
    ]
    for load in loads:
        load.start()

    ids = route_ids[...]
    lanes = round_up(n_ep, 128)
    expert_iota = lax.broadcasted_iota(jnp.int32, (tokens, lanes), 1)
    named = [(ids[:, k : k + 1] == expert_iota).astype(F32) for k in range(ids.shape[1])]
    counts = functools.reduce(lambda a, b: a + b, named)
    lower = (
        lax.broadcasted_iota(jnp.int32, (tokens, tokens), 0)
        > lax.broadcasted_iota(jnp.int32, (tokens, tokens), 1)
    ).astype(F32)
    before = jnp.dot(lower.astype(BF16), counts.astype(BF16), preferred_element_type=F32)
    slot_iota = lax.broadcasted_iota(jnp.int32, (tokens, n_ep * slots), 1)
    for k in range(ids.shape[1]):
        rank = jnp.sum(before * named[k], axis=1, keepdims=True)
        slot = ids[:, k : k + 1] * slots + rank.astype(jnp.int32)
        pick[k] = (slot_iota == slot).astype(F32).astype(BF16)

    step = 32
    normed_parts = []
    for start in range(0, tokens, step):
        wide = expert_in[start : start + step, :].astype(F32)
        scaling = lax.rsqrt(jnp.mean(wide * wide, axis=1, keepdims=True) + 1e-06)
        block = expert_in[start : start + step, own].astype(F32)
        normed_parts.append((block * scaling * gain[:, own]).astype(BF16))
    normed = jnp.concatenate(normed_parts, axis=0)
    hits = functools.reduce(lambda a, b: a + b, [pick[k] for k in range(ids.shape[1])])
    sent = lax.dot_general(
        hits, normed, (((0,), (0,)), ((), ())), preferred_element_type=F32
    ).astype(BF16)
    for e in range(n_ep):
        send_rows[e] = sent[e * slots : (e + 1) * slots]

    pl.semaphore_wait(barrier, n_ep - 1 + n_tp - 1)

    def position(p):
        return rows.at[pl.ds(p * slots, slots), own]

    dispatches = {
        p: remote(
            send_rows.at[partner(ep, p)],
            position(p),
            disp_send_sem.at[p],
            disp_recv_sem.at[p],
            ep_peer(p),
        )
        for p in range(1, n_ep)
    }
    for p in range(1, n_ep):
        dispatches[p].start()
    rows[0:slots, own] = send_rows[ep]

    seq = gate_in.shape[0]
    tap_count = taps.shape[0]
    edge = halo.shape[0]
    product = gate_in[...].astype(F32) * conv_values[...].astype(F32)
    padded[edge:, :] = product
    product_tail[...] = product[seq - edge :]
    halo_copy = remote(
        product_tail, halo, halo_sem.at[0], halo_sem.at[1], {"ep": (ep + 1) % n_ep}
    )
    halo_copy.start()
    loads[0].wait()
    halo_copy.wait()
    padded[0:edge, :] = halo[...] * (ep > 0).astype(F32)
    convolved = taps[0:1, :] * padded[edge - tap_count + 1 : edge - tap_count + 1 + seq, :]
    for offset in range(1, tap_count):
        base = edge - tap_count + 1 + offset
        convolved = convolved + taps[offset : offset + 1, :] * padded[base : base + seq, :]
    branch = (gate_out[...].astype(F32) * convolved).astype(BF16)
    mix_copies = {}
    for q in list(range(1, n_tp)) + [0]:
        columns = pl.ds(pl.multiple_of(partner(tp, q) * width, width), width)
        mix_part[q] = jnp.dot(branch, mixer_w[:, columns], preferred_element_type=F32).astype(BF16)
        if q:
            mix_copies[q] = remote(
                mix_part.at[q], mix_recv.at[q], mix_send_sem.at[q], mix_recv_sem.at[q], tp_peer(q)
            )
            mix_copies[q].start()

    gathers = {}

    def send_gather(j):
        for p in range(j * group, (j + 1) * group):
            if p:
                dispatches[p].wait_recv()
        block = rows.at[pl.ds(j * span, span), own]
        for q in range(1, n_tp):
            gathers[j, q] = remote(
                block, block, gather_send_sem.at[j, q], gather_recv_sem.at[j, q], tp_peer(q)
            )
            gathers[j, q].start()

    tile = min(256, gate_w.shape[1])
    part_copies = {}
    back_copies = {}

    def run_expert(j):
        for q in range(1, n_tp):
            gathers[j, q].wait_recv()
        here = slice(j * span, (j + 1) * span)

        @pl.loop(0, gate_w.shape[1] // tile)
        def _(i):
            columns = pl.ds(pl.multiple_of(i * tile, tile), tile)
            gate = jnp.dot(rows[here, :], gate_w[:, columns], preferred_element_type=F32)
            up = jnp.dot(rows[here, :], up_w[:, columns], preferred_element_type=F32)
            hidden[:, columns] = (gate / (1.0 + jnp.exp(-gate)) * up).astype(BF16)

        if j == 0:
            loads[3].wait()
        for q in list(range(1, n_tp)) + [0]:
            columns = pl.ds(pl.multiple_of(partner(tp, q) * width, width), width)
            part[j, q] = jnp.dot(hidden[...], down_w[:, columns], preferred_element_type=F32).astype(BF16)
            if q:
                part_copies[j, q] = remote(
                    part.at[j, q],
                    recv.at[j, q],
                    part_send_sem.at[j, q],
                    part_recv_sem.at[j, q],
                    tp_peer(q),
                )
                part_copies[j, q].start()

    def send_back(j):
        total = part[j, 0].astype(F32)
        for q in range(1, n_tp):
            part_copies[j, q].wait_recv()
            total = total + recv[j, q].astype(F32)
        summed[pl.ds(j * span, span), :] = total.astype(BF16)
        for p in range(j * group, (j + 1) * group):
            block = summed.at[pl.ds(p * slots, slots), :]
            if p:
                back_copies[p] = remote(
                    block, back.at[pl.ds(ep * slots, slots), :], back_send_sem.at[p], back_recv_sem.at[p], ep_peer(p)
                )
                back_copies[p].start()
            else:
                back[pl.ds(ep * slots, slots), :] = block[...]

    for j in range(chunks):
        send_gather(j)
        if j == 0:
            loads[1].wait()
            loads[2].wait()
        if j > 0:
            run_expert(j - 1)
        if j > 1:
            send_back(j - 2)
    run_expert(chunks - 1)
    if chunks > 1:
        send_back(chunks - 2)

    total = mix_part[0].astype(F32)
    for q in range(1, n_tp):
        mix_copies[q].wait_recv()
        total = total + mix_recv[q].astype(F32)
    mixed[...] = total.astype(BF16)

    send_back(chunks - 1)

    for p in range(1, n_ep):
        back_copies[p].wait_recv()
    weights = scores[...]
    weights = weights / jnp.sum(weights, axis=1, keepdims=True)
    mix = None
    for k in range(ids.shape[1]):
        picked = jnp.dot(pick[k], back[...], preferred_element_type=F32)
        term = weights[:, k : k + 1] * picked
        mix = term if mix is None else mix + term
    expert_mix[...] = mix.astype(BF16)

    for copies in (dispatches, mix_copies, gathers, part_copies, back_copies):
        for copy in copies.values():
            copy.wait_send()


def shards(
    gate_out,
    gate_in,
    conv_values,
    conv_taps,
    mixer_proj,
    expert_in,
    norm_gain,
    route_ids,
    route_scores,
    gate_proj,
    up_proj,
    down_proj,
):
    n_ep, n_tp = lax.axis_size("ep"), lax.axis_size("tp")
    tokens, model = expert_in.shape
    choices = route_ids.shape[1]
    capacity = max(2, (4 * tokens * choices + 3 * n_ep - 1) // (3 * n_ep))
    slots = round_up(capacity, 16)
    width = model // n_tp
    group = 2 if n_ep % 2 == 0 else 1
    while group * slots < 128 and group * 2 <= n_ep:
        group *= 2
    chunks = n_ep // group
    span = group * slots
    seq, channels = gate_out.shape
    hidden_units = gate_proj.shape[2]
    vmem = pl.BlockSpec(memory_space=pltpu.VMEM)
    hbm = pl.BlockSpec(memory_space=pl.ANY)
    dma = pltpu.SemaphoreType.DMA
    call = pl.pallas_call(
        functools.partial(kernel, (n_ep, n_tp, slots, width)),
        out_shape=(
            jax.ShapeDtypeStruct((seq, width), BF16),
            jax.ShapeDtypeStruct((tokens, width), BF16),
        ),
        in_specs=[vmem] * 8 + [hbm] * 4,
        out_specs=(vmem, vmem),
        scratch_shapes=[
            pltpu.VMEM((channels, model), BF16),
            pltpu.VMEM((model, hidden_units), BF16),
            pltpu.VMEM((model, hidden_units), BF16),
            pltpu.VMEM((hidden_units, model), BF16),
            pltpu.VMEM((seq + 8, channels), F32),
            pltpu.VMEM((8, channels), F32),
            pltpu.VMEM((8, channels), F32),
            pltpu.VMEM((n_tp, seq, width), BF16),
            pltpu.VMEM((n_tp, seq, width), BF16),
            pltpu.VMEM((n_ep, slots, width), BF16),
            pltpu.VMEM((n_ep * slots, model), BF16),
            pltpu.VMEM((span, hidden_units), BF16),
            pltpu.VMEM((chunks, n_tp, span, width), BF16),
            pltpu.VMEM((chunks, n_tp, span, width), BF16),
            pltpu.VMEM((n_ep * slots, width), BF16),
            pltpu.VMEM((n_ep * slots, width), BF16),
            pltpu.VMEM((choices, tokens, n_ep * slots), BF16),
            dma((4,)),
            dma((2,)),
            dma((n_tp,)),
            dma((n_tp,)),
            dma((n_ep,)),
            dma((n_ep,)),
            dma((chunks, n_tp)),
            dma((chunks, n_tp)),
            dma((chunks, n_tp)),
            dma((chunks, n_tp)),
            dma((n_ep,)),
            dma((n_ep,)),
        ],
        compiler_params=pltpu.CompilerParams(
            collective_id=0, has_side_effects=True, vmem_limit_bytes=60 * 1024 * 1024
        ),
    )
    return call(
        gate_out,
        gate_in,
        conv_values,
        conv_taps,
        expert_in,
        norm_gain.reshape(1, model),
        route_ids,
        route_scores,
        mixer_proj,
        gate_proj.reshape(model, hidden_units),
        up_proj.reshape(model, hidden_units),
        down_proj.reshape(hidden_units, model),
    )


def solution(mesh):
    placed = (
        P("ep", "tp"),
        P("ep", "tp"),
        P("ep", "tp"),
        P(None, "tp"),
        P("tp", None),
        P("ep", None),
        P(),
        P("ep", None),
        P("ep", None),
        P("ep", None, "tp"),
        P("ep", None, "tp"),
        P("ep", "tp", None),
    )
    return jax.shard_map(
        shards,
        mesh=mesh,
        in_specs=placed,
        out_specs=(P("ep", "tp"), P("ep", "tp")),
        check_vma=False,
    )
```

time: 187 us -> 119 us (0.64)
  Pallas kernels: 0 us -> 111 us
  waiting for transfers between devices: 100 us -> 0 us
  matrix products: 23.7 us -> 0 us
  blocking collectives: 21.4 us -> 0 us
  between operations: 14 us -> 0.64 us
  other arithmetic: 7.69 us -> 0 us
  starting transfers between devices: 7.16 us -> 0 us
  local copies, waits for them, and re-layouts: 10.9 us -> 6.29 us
    pallas_call x0 -> x1, Pallas kernels: none -> 111 us  [shards(): call(gate_out, gate_in, conv_values, conv_taps, expert_in, norm_gain.resh...]
    all_gather x1 -> x0, waiting for transfers between devices: 42.6 us -> none  [shards(): piece = lax.all_gather(arrived, 'tp', axis=1, tiled=True)]
    reduce_scatter x2 -> x0, waiting for transfers between devices: 39.3 us -> none  [the longest x1 34.5 us: shards(): lax.psum_scatter(partial_out.astype(jnp.bfloat16), 'tp', scatter_dimensio...]
    dot_general x4 -> x0, matrix products: 23.7 us -> none  [the longest x1 13 us: shards(): jnp.einsum('secf,efd->secd', hidden, down_proj, preferred_element_type=jn...]
    all_to_all x1 -> x0, blocking collectives: 21.4 us -> none  [shards(): lax.all_to_all(sent, 'ep', split_axis=0, concat_axis=0, tiled=True)]
    all_to_all x1 -> x0, waiting for transfers between devices: 15.6 us -> none  [shards(): lax.all_to_all(summed, 'ep', split_axis=0, concat_axis=0, tiled=True)]
    all_to_all x1 -> x0, starting transfers between devices: 5.12 us -> none  [shards(): lax.all_to_all(summed, 'ep', split_axis=0, concat_axis=0, tiled=True)]
    unnamed x17 -> x4, local copies, waits for them, and re-layouts: 1.85 us -> 6.29 us
  transfers between devices with their start and end apart: 5 -> 0, of which waited for: 5 -> 0; matrix products, arithmetic and copies ran while one was open for 4% -> 0% of each run, Pallas kernels for 0% -> 0%
where the time goes in v1:
time: 119 us; the launch traced here: 118 us
  Pallas kernels  111 us (93%)
  local copies, waits for them, and re-layouts  6.29 us (5%)
    pallas_call x1, Pallas kernels, shards(): call(gate_out, gate_in, conv_values, conv_taps, expert_in, norm_gain.resh...  111 us
    unnamed x4, local copies, waits for them, and re-layouts  6.29 us

profile of v1, /device:TPU:16, one launch (start us, length us, event | category | flops | bytes accessed | tf_op | source)
XLA Modules:
  0.0 118.1 jit_solution(15432262856066936407)
XLA Ops:
  0.6 1.5 %copy.14.route_ids = s32[256,2]{1,0:T(8,128)} copy(s32[256,2]{0,1:T(2,128)} %param.19) | data formatting | bytes 4096 | tf_op args[7]
  2.1 1.5 %copy.15.scores = f32[256,2]{1,0:T(8,128)} copy(f32[256,2]{0,1:T(2,128)} %param.20) | data formatting | bytes 4096 | tf_op args[8]
  3.6 111.1 %shard_map.131 = (bf16[256,512]{1,0:T(8,128)(2,1)}, bf16[256,512]{1,0:T(8,128)(2,1)}) custom-call(bf16[256,256]{1,0:T(8,128)(2,1)} %gate_out.1, bf16[256,256]{1,0:T(8,128)(2,1)} %gate_in.1, bf16[256,256]{1,0:T(8,128)(2,1)} %conv_values.1, f32[3,256]{1,0:T(4,128)} %taps.1, bf16[256,2048]{1,0:T(8,128)(2,1)} %expert_in.1, f32[1,2048]{1,0:T(1,128)} %bitcast.7, ...), custom_call_target="tpu_custom_call" | custom-call | tf_op jit(solution)/shard_map/pallas_call | solution.py:364
  114.7 1.7 %copy.18 = bf16[256,512]{1,0:T(8,128)(2,1)} copy(bf16[256,512]{1,0:T(8,128)(2,1)} %get-tuple-element.4) | data formatting | bytes 524288
  116.4 1.7 %copy.19 = bf16[256,512]{1,0:T(8,128)(2,1)} copy(bf16[256,512]{1,0:T(8,128)(2,1)} %get-tuple-element.5) | data formatting | bytes 524288

commit v2 on v1

--- a/solution.py
+++ b/solution.py
@@ -22,6 +22,13 @@
             index = index + bit - 2 * bit * ((index // bit) % 2)
         bit *= 2
     return index
+
+
+def row_steps(n_tp):
+    inner = 1
+    while inner * inner < n_tp:
+        inner *= 2
+    return list(range(1, inner)), list(range(inner, n_tp, inner))
 
 
 def kernel(
@@ -159,7 +166,7 @@
         )
         for p in range(1, n_ep)
     }
-    for p in range(1, n_ep):
+    for p in list(range(group, n_ep)) + list(range(1, group)):
         dispatches[p].start()
     rows[0:slots, own] = send_rows[ep]
 
@@ -181,37 +188,112 @@
         base = edge - tap_count + 1 + offset
         convolved = convolved + taps[offset : offset + 1, :] * padded[base : base + seq, :]
     branch = (gate_out[...].astype(F32) * convolved).astype(BF16)
-    mix_copies = {}
-    for q in list(range(1, n_tp)) + [0]:
+    x_steps, y_steps = row_steps(n_tp)
+    halves = ((0, x_steps, y_steps), (1, y_steps, x_steps))
+
+    class ReduceScatter:
+
+        def __init__(self, parts, arrivals, send_sems, recv_sems):
+            self.parts, self.arrivals = parts, arrivals
+            self.sems = (send_sems, recv_sems)
+            self.copies = {}
+            self.half = parts.shape[1] // 2
+
+        def cut(self, ref, q, half):
+            return ref.at[q, pl.ds(half * self.half, self.half), :]
+
+        def send(self, q, half, to):
+            copy = remote(
+                self.cut(self.parts, q, half),
+                self.cut(self.arrivals, q, half),
+                self.sems[0].at[q, half],
+                self.sems[1].at[q, half],
+                tp_peer(to),
+            )
+            copy.start()
+            self.copies[q, half] = copy
+
+        def first(self, q):
+            for half, near, far in halves:
+                for step in near:
+                    if q - step in [0] + far:
+                        self.send(q, half, step)
+
+        def gathered(self, q, half, near):
+            total = self.cut(self.parts, q, half)[...].astype(F32)
+            for step in near:
+                self.copies[step + q, half].wait_recv()
+                total = total + self.cut(self.arrivals, step + q, half)[...].astype(F32)
+            return total
+
+        def second(self):
+            for half, near, far in halves:
+                for q in far:
+                    total = self.gathered(q, half, near)
+                    self.parts[q, half * self.half : (half + 1) * self.half, :] = total.astype(BF16)
+                    self.send(q, half, q)
+
+        def finish(self, half):
+            _, near, far = halves[half]
+            total = self.gathered(0, half, near)
+            for q in far:
+                self.copies[q, half].wait_recv()
+                total = total + self.cut(self.arrivals, q, half)[...].astype(F32)
+            return total.astype(BF16)
+
+    order = [q for q in range(n_tp - 1, -1, -1)]
+
+    mix_sum = ReduceScatter(mix_part, mix_recv, mix_send_sem, mix_recv_sem)
+    for q in order:
         columns = pl.ds(pl.multiple_of(partner(tp, q) * width, width), width)
         mix_part[q] = jnp.dot(branch, mixer_w[:, columns], preferred_element_type=F32).astype(BF16)
         if q:
-            mix_copies[q] = remote(
-                mix_part.at[q], mix_recv.at[q], mix_send_sem.at[q], mix_recv_sem.at[q], tp_peer(q)
-            )
-            mix_copies[q].start()
+            mix_sum.first(q)
 
     gathers = {}
+
+    def columns_of(q):
+        return pl.ds(pl.multiple_of(partner(tp, q) * width, width), width)
+
+    def send_block(j, q, first_row, row_count, half, to):
+        block = rows.at[pl.ds(first_row, row_count), columns_of(q)]
+        copy = remote(
+            block,
+            block,
+            gather_send_sem.at[j, q ^ to, half],
+            gather_recv_sem.at[j, q ^ to, half],
+            tp_peer(to),
+        )
+        copy.start()
+        gathers[j, q ^ to, half] = copy
 
     def send_gather(j):
         for p in range(j * group, (j + 1) * group):
             if p:
                 dispatches[p].wait_recv()
-        block = rows.at[pl.ds(j * span, span), own]
-        for q in range(1, n_tp):
-            gathers[j, q] = remote(
-                block, block, gather_send_sem.at[j, q], gather_recv_sem.at[j, q], tp_peer(q)
-            )
-            gathers[j, q].start()
+        for step in x_steps + y_steps:
+            send_block(j, 0, j * span, span, 0, step)
+
+    def forward(j):
+        for step in x_steps + y_steps:
+            gathers[j, step, 0].wait_recv()
+        for half, near, far in halves:
+            for via in near:
+                for to in far:
+                    send_block(j, via, j * span + half * (span // 2), span // 2, half, to)
 
     tile = min(256, gate_w.shape[1])
-    part_copies = {}
+    sums = {}
     back_copies = {}
 
-    def run_expert(j):
-        for q in range(1, n_tp):
-            gathers[j, q].wait_recv()
+    def run_expert(j, first):
+        for (at, q, half), copy in list(gathers.items()):
+            if at == j and q not in x_steps + y_steps:
+                copy.wait_recv()
         here = slice(j * span, (j + 1) * span)
+        if first:
+            loads[1].wait()
+            loads[2].wait()
 
         @pl.loop(0, gate_w.shape[1] // tile)
         def _(i):
@@ -220,57 +302,58 @@
             up = jnp.dot(rows[here, :], up_w[:, columns], preferred_element_type=F32)
             hidden[:, columns] = (gate / (1.0 + jnp.exp(-gate)) * up).astype(BF16)
 
-        if j == 0:
+        if first:
             loads[3].wait()
-        for q in list(range(1, n_tp)) + [0]:
-            columns = pl.ds(pl.multiple_of(partner(tp, q) * width, width), width)
-            part[j, q] = jnp.dot(hidden[...], down_w[:, columns], preferred_element_type=F32).astype(BF16)
+        sums[j] = ReduceScatter(part.at[j], recv.at[j], part_send_sem.at[j], part_recv_sem.at[j])
+        for q in order:
+            part[j, q] = jnp.dot(
+                hidden[...], down_w[:, columns_of(q)], preferred_element_type=F32
+            ).astype(BF16)
             if q:
-                part_copies[j, q] = remote(
-                    part.at[j, q],
-                    recv.at[j, q],
-                    part_send_sem.at[j, q],
-                    part_recv_sem.at[j, q],
-                    tp_peer(q),
-                )
-                part_copies[j, q].start()
+                sums[j].first(q)
 
     def send_back(j):
-        total = part[j, 0].astype(F32)
-        for q in range(1, n_tp):
-            part_copies[j, q].wait_recv()
-            total = total + recv[j, q].astype(F32)
-        summed[pl.ds(j * span, span), :] = total.astype(BF16)
+        for half in range(2):
+            summed[pl.ds(j * span + half * (span // 2), span // 2), :] = sums[j].finish(half)
         for p in range(j * group, (j + 1) * group):
             block = summed.at[pl.ds(p * slots, slots), :]
             if p:
                 back_copies[p] = remote(
-                    block, back.at[pl.ds(ep * slots, slots), :], back_send_sem.at[p], back_recv_sem.at[p], ep_peer(p)
+                    block,
+                    back.at[pl.ds(ep * slots, slots), :],
+                    back_send_sem.at[p],
+                    back_recv_sem.at[p],
+                    ep_peer(p),
                 )
                 back_copies[p].start()
             else:
                 back[pl.ds(ep * slots, slots), :] = block[...]
 
-    for j in range(chunks):
+    turns = list(range(1, chunks)) + [0]
+    for i, j in enumerate(turns):
         send_gather(j)
-        if j == 0:
-            loads[1].wait()
-            loads[2].wait()
-        if j > 0:
-            run_expert(j - 1)
-        if j > 1:
-            send_back(j - 2)
-    run_expert(chunks - 1)
-    if chunks > 1:
-        send_back(chunks - 2)
-
-    total = mix_part[0].astype(F32)
-    for q in range(1, n_tp):
-        mix_copies[q].wait_recv()
-        total = total + mix_recv[q].astype(F32)
-    mixed[...] = total.astype(BF16)
-
-    send_back(chunks - 1)
+        if i == 0:
+            mix_sum.second()
+        if i > 0:
+            forward(turns[i - 1])
+        if i > 1:
+            run_expert(turns[i - 2], i == 2)
+        if i > 2:
+            sums[turns[i - 3]].second()
+        if i > 3:
+            send_back(turns[i - 4])
+    forward(turns[-1])
+    for i in range(chunks - 2, chunks):
+        run_expert(turns[i], i == 0)
+        sums[turns[i - 1]].second()
+        if i > 1:
+            send_back(turns[i - 2])
+    for half in range(2):
+        rest = mixed.shape[0] // 2
+        mixed[half * rest : (half + 1) * rest, :] = mix_sum.finish(half)
+    sums[turns[-1]].second()
+    send_back(turns[-2])
+    send_back(turns[-1])
 
     for p in range(1, n_ep):
         back_copies[p].wait_recv()
@@ -283,7 +366,9 @@
         mix = term if mix is None else mix + term
     expert_mix[...] = mix.astype(BF16)
 
-    for copies in (dispatches, mix_copies, gathers, part_copies, back_copies):
+    started = [dispatches, gathers, back_copies, mix_sum.copies]
+    started += [total.copies for total in sums.values()]
+    for copies in started:
         for copy in copies.values():
             copy.wait_send()
 
@@ -346,14 +431,14 @@
             pltpu.VMEM((choices, tokens, n_ep * slots), BF16),
             dma((4,)),
             dma((2,)),
-            dma((n_tp,)),
-            dma((n_tp,)),
+            dma((n_tp, 2)),
+            dma((n_tp, 2)),
             dma((n_ep,)),
             dma((n_ep,)),
-            dma((chunks, n_tp)),
-            dma((chunks, n_tp)),
-            dma((chunks, n_tp)),
-            dma((chunks, n_tp)),
+            dma((chunks, n_tp, 2)),
+            dma((chunks, n_tp, 2)),
+            dma((chunks, n_tp, 2)),
+            dma((chunks, n_tp, 2)),
             dma((n_ep,)),
             dma((n_ep,)),
         ],

time: 119 us -> 98.2 us (0.83)
  Pallas kernels: 111 us -> 91.1 us
    pallas_call x1, Pallas kernels: 111 us -> 91.1 us  [shards(): call(gate_out, gate_in, conv_values, conv_taps, expert_in, norm_gain.resh...]
where the time goes in v2:
time: 98.2 us; the launch traced here: 98 us
  Pallas kernels  91.1 us (93%)
  local copies, waits for them, and re-layouts  6.29 us (6%)
    pallas_call x1, Pallas kernels, shards(): call(gate_out, gate_in, conv_values, conv_taps, expert_in, norm_gain.resh...  91.1 us
    unnamed x4, local copies, waits for them, and re-layouts  6.29 us

profile of v2, /device:TPU:16, one launch (start us, length us, event | category | flops | bytes accessed | tf_op | source)
XLA Modules:
  0.0 98.0 jit_solution(3563834028463798013)
XLA Ops:
  0.6 1.5 %copy.14.route_ids = s32[256,2]{1,0:T(8,128)} copy(s32[256,2]{0,1:T(2,128)} %param.19) | data formatting | bytes 4096 | tf_op args[7]
  2.1 1.5 %copy.15.scores = f32[256,2]{1,0:T(8,128)} copy(f32[256,2]{0,1:T(2,128)} %param.20) | data formatting | bytes 4096 | tf_op args[8]
  3.6 91.1 %shard_map.131 = (bf16[256,512]{1,0:T(8,128)(2,1)}, bf16[256,512]{1,0:T(8,128)(2,1)}) custom-call(bf16[256,256]{1,0:T(8,128)(2,1)} %gate_out.1, bf16[256,256]{1,0:T(8,128)(2,1)} %gate_in.1, bf16[256,256]{1,0:T(8,128)(2,1)} %conv_values.1, f32[3,256]{1,0:T(4,128)} %taps.1, bf16[256,2048]{1,0:T(8,128)(2,1)} %expert_in.1, f32[1,2048]{1,0:T(1,128)} %bitcast.7, ...), custom_call_target="tpu_custom_call" | custom-call | tf_op jit(solution)/shard_map/pallas_call | solution.py:449
  94.6 1.7 %copy.18 = bf16[256,512]{1,0:T(8,128)(2,1)} copy(bf16[256,512]{1,0:T(8,128)(2,1)} %get-tuple-element.4) | data formatting | bytes 524288
  96.3 1.7 %copy.19 = bf16[256,512]{1,0:T(8,128)(2,1)} copy(bf16[256,512]{1,0:T(8,128)(2,1)} %get-tuple-element.5) | data formatting | bytes 524288
